TPU v7x, 32 devices: a whole 2x2x4 slice. The times are simulated.
32 devices in a mesh: grp: 2 (over x), tp: 16 (over z, y, core).
Axes of the slice: x: 2, y: 2, z: 4, core: 2. Of those that a mesh axis runs over, the one named last changes fastest.
Arguments:
- stream_in: bfloat16 [64, 4, 4096], P('grp'), parts along dimension 0, may hold values from -6 to 6
- state_in: float32 [2, 64, 8, 256, 256], P(None, 'grp', None, 'tp'), parts along dimension 1, may hold values from -0.8 to 0.8
- norm_gain: bfloat16 [2, 4096], replicated, may hold values from 0.099609375 to 1.8984375
- query_weight: bfloat16 [2, 4096, 2048], P(None, None, 'tp'), may hold values from -0.09375 to 0.09375
- key_weight: bfloat16 [2, 4096, 2048], P(None, None, 'tp'), may hold values from -0.09375 to 0.09375
- value_weight: bfloat16 [2, 4096, 8, 256], P(None, None, None, 'tp'), as said below
- gate_weight: bfloat16 [2, 4096, 8, 256], P(None, None, None, 'tp'), may hold values from -0.09375 to 0.09375
- group_gain: bfloat16 [2, 8, 256], P(None, None, 'tp'), may hold values from 0.099609375 to 1.8984375
- output_weight: bfloat16 [2, 8, 256, 4096], P(None, None, 'tp'), may hold values from -0.375 to 0.375
Outputs:
- stream_out: bfloat16 [64, 4, 4096], P('grp', None, 'tp'), parts along dimension 0
- state_out: float32 [2, 64, 8, 256, 256], P(None, 'grp', None, 'tp'), parts along dimension 1
There are 2 independent parts, one for each index of `grp`. A program takes and returns all parts, laid end to end along the dimension named above; an argument that names none is the same for every part. Nothing has to cross between parts.
Inputs may be any that keep to these rules, and one draw needn't show every extreme that they name: `value_weight`: real values; column scales of the value projection differ.
All inputs are finite; a program needn't handle non-finite values.
Results may differ from a plain program's by a relative error of at most 0.024.
Values may be sent and summed in bfloat16 or wider, within the bound.
No kernel may reach another device: no remote copies, remote signals or barrier semaphores. Data moves between devices by JAX's collectives and lax.ppermute only.
A program may use at most 64 MiB of HBM per device.

v0:
```python
import jax
import jax.numpy as jnp
from jax import lax
from jax.sharding import PartitionSpec as P

HEAD_DIM = 256
PAST = 1024
EPS_RMS = 1e-06
EPS_GROUP = 1e-05
ROTARY_BASE = 10000.0


def log_decays(count):
    return jnp.log(1.0 - jnp.power(2.0, -5.0 - jnp.arange(count, dtype=jnp.float32)))


def decay_tables(log_gamma, count):
    steps = jnp.arange(count, dtype=jnp.float32)
    gap = steps[:, None] - steps[None, :]
    intra = jnp.where(
        gap[None] >= 0, jnp.exp(log_gamma[:, None, None] * jnp.maximum(gap, 0.0)[None]), 0.0
    )
    q_decay = jnp.exp(log_gamma[None, :] * (steps[:, None] + 1.0))
    k_decay = jnp.exp(log_gamma[None, :] * (count - 1.0 - steps[:, None]))
    block_decay = jnp.exp(log_gamma * count)
    return (intra, q_decay, k_decay, block_decay)


def rotate(values, offset):
    half_dim = values.shape[-1] // 2
    freqs = jnp.power(
        ROTARY_BASE, -jnp.arange(half_dim, dtype=jnp.float32) * (2.0 / values.shape[-1])
    )
    places = (offset + jnp.arange(values.shape[1])).astype(jnp.float32)
    angles = places[:, None] * freqs[None, :]
    cosine = jnp.cos(angles)[None, :, None, :]
    sine = jnp.sin(angles)[None, :, None, :]
    first = values[..., :half_dim]
    second = values[..., half_dim:]
    return jnp.concatenate(
        [first * cosine - second * sine, second * cosine + first * sine], axis=-1
    )


def local(
    stream_in,
    state_in,
    norm_gain,
    query_weight,
    key_weight,
    value_weight,
    gate_weight,
    group_gain,
    output_weight,
):
    seqs, new_tok, width = stream_in.shape
    heads, local_dim = (value_weight.shape[2], value_weight.shape[3])
    head_dim = HEAD_DIM
    log_gamma = log_decays(heads)
    intra, q_decay, k_decay, block_decay = decay_tables(log_gamma, new_tok)
    highest = lax.Precision.HIGHEST
    share_cols = width // lax.axis_size("tp")
    col_start = lax.axis_index("tp") * share_cols
    layers = state_in.shape[0]
    stream = stream_in
    stream_share = stream_in
    new_states = []
    for layer_no in range(layers):
        stream_f = stream.astype(jnp.float32)
        normed = stream_f * lax.rsqrt(
            jnp.mean(stream_f * stream_f, axis=-1, keepdims=True) + EPS_RMS
        )
        normed = (normed * norm_gain[layer_no].astype(jnp.float32)).astype(jnp.bfloat16)
        flat = normed.reshape(seqs * new_tok, width)
        query_part = jnp.dot(flat, query_weight[layer_no], preferred_element_type=jnp.float32)
        query_part = query_part.astype(jnp.bfloat16).reshape(seqs, new_tok, -1)
        key_part = jnp.dot(flat, key_weight[layer_no], preferred_element_type=jnp.float32)
        key_part = key_part.astype(jnp.bfloat16).reshape(seqs, new_tok, -1)

        def project_local(weight):
            result = jnp.dot(
                flat, weight.reshape(width, heads * local_dim), preferred_element_type=jnp.float32
            )
            result = lax.optimization_barrier(result.astype(jnp.bfloat16))
            return result.astype(jnp.float32).reshape(seqs, new_tok, heads, local_dim)

        values_f = project_local(value_weight[layer_no])
        gates_f = project_local(gate_weight[layer_no])
        queries, key_rows = (
            lax.all_gather(query_part, "tp", axis=2, tiled=True),
            lax.all_gather(key_part, "tp", axis=2, tiled=True),
        )
        queries = queries.astype(jnp.float32).reshape(seqs, new_tok, heads, head_dim)
        key_rows = key_rows.astype(jnp.float32).reshape(seqs, new_tok, heads, head_dim)
        rot_q = rotate(queries, PAST)
        rot_k = rotate(key_rows, PAST) * head_dim ** (-0.5)
        scores = jnp.einsum("bthd,bshd->bhts", rot_q, rot_k, precision=highest) * intra[None]
        inner = jnp.einsum("bhts,bshe->bthe", scores, values_f, precision=highest)
        state = state_in[layer_no]
        carried = (
            jnp.einsum("bthd,bhed->bthe", rot_q, state, precision=highest)
            * q_decay[None, :, :, None]
        )
        mixed = inner + carried
        new_state = state * block_decay[None, :, None, None] + jnp.einsum(
            "bthe,bthd->bhed", values_f, rot_k * k_decay[None, :, :, None], precision=highest
        )
        new_states.append(new_state)
        totals, squares = lax.psum((jnp.sum(mixed, axis=-1), jnp.sum(mixed * mixed, axis=-1)), "tp")
        mean_o = (totals / head_dim)[..., None]
        var_o = (squares / head_dim)[..., None] - mean_o * mean_o
        normal = (
            (mixed - mean_o)
            * lax.rsqrt(var_o + EPS_GROUP)
            * group_gain[layer_no].astype(jnp.float32)[None, None]
        )
        gated = (jax.nn.silu(gates_f) * normal).astype(jnp.bfloat16)
        partial_out = jnp.dot(
            gated.reshape(seqs * new_tok, heads * local_dim),
            output_weight[layer_no].reshape(heads * local_dim, width),
            preferred_element_type=jnp.float32,
        ).reshape(seqs, new_tok, width)
        share_out = lax.psum_scatter(partial_out, "tp", scatter_dimension=2, tiled=True)
        own_cols = lax.dynamic_slice_in_dim(stream, col_start, share_cols, 2)
        stream_share = (own_cols.astype(jnp.float32) + share_out).astype(jnp.bfloat16)
        if layer_no + 1 < layers:
            stream = lax.all_gather(stream_share, "tp", axis=2, tiled=True)
    result = stream_share
    return (result, jnp.stack(new_states))


def solution(mesh):
    in_specs = (
        P("grp", None, None),
        P(None, "grp", None, "tp", None),
        P(),
        P(None, None, "tp"),
        P(None, None, "tp"),
        P(None, None, None, "tp"),
        P(None, None, None, "tp"),
        P(None, None, "tp"),
        P(None, None, "tp", None),
    )
    out_specs = (P("grp", None, "tp"), P(None, "grp", None, "tp", None))
    return jax.shard_map(local, mesh=mesh, in_specs=in_specs, out_specs=out_specs, check_vma=False)
```

profile of v0, /device:TPU:0, one launch (start us, length us, event | category | flops | bytes accessed | tf_op | source)
XLA Modules:
  0.0 433.5 jit_solution(2907268632619906550)
XLA Ops:
  7.3 0.7 bitcast_convert_fusion
  8.0 1.8 fusion.10
  9.9 0.8 slice_convert_fusion
  10.7 1.9 fusion.12
  12.9 1.8 convolution_convert_fusion.4
  14.8 0.4 convolution_convert_fusion.5
  15.2 24.6 %all_gather.15 = bf16[32,4,2048]{2,1,0:T(4,128)(2,1)S(1)} all-gather(bf16[32,4,128]{2,1,0:T(4,128)(2,1)S(1)} %bitcast.115), channel_id=1, replica_groups=mesh['grp'=2,'tp'=16] {'tp'}, dimensions={2}, use_global_device_ids=true | all-gather | bytes 557056 | tf_op jit(solution)/shard_map/all_gather | solution.py:90
  39.8 19.0 %all_gather.16 = bf16[32,4,2048]{2,1,0:T(4,128)(2,1)S(1)} all-gather(bf16[32,4,128]{2,1,0:T(4,128)(2,1)S(1)} %bitcast.114), channel_id=1, replica_groups=mesh['grp'=2,'tp'=16] {'tp'}, dimensions={2}, use_global_device_ids=true | all-gather | bytes 557056 | tf_op jit(solution)/shard_map/all_gather | solution.py:91
  59.3 0.6 multiply_subtract_fusion.2
  59.9 6.9 %fusion.4 = f32[32,8,4,16]{3,2,1,0:T(4,128)} fusion(f32[2,32,8,16,256]{4,3,2,1,0:T(8,128)} %param.10, f32[32,4,8,128]{3,1,2,0:T(4,128)S(1)} %get-tuple-element.46, f32[32,4,8,128]{3,1,2,0:T(4,128)S(1)} %get-tuple-element.47), kind=kOutput, calls=%fused_computation.7 | convolution fusion | flops 50593792 | bytes 5308416 | tf_op jit(solution)/shard_map/bthd,bhed->bthe/dot_general | solution.py:101
  66.8 2.0 copy.76
  68.9 2.7 fusion.56
  71.5 0.4 convolution_convert_fusion.6
  72.3 2.3 convolution_multiply_fusion.1
  74.6 1.0 fusion.38
  75.9 2.7 fusion.55
  78.7 0.4 convolution_convert_fusion.7
  79.6 1.8 fusion.54
  81.6 59.1 %all-reduce.1 = (f32[32,4,8]{0,2,1:T(8,128)S(1)}, f32[32,4,8]{0,2,1:T(8,128)S(1)}) all-reduce(f32[32,4,8]{0,2,1:T(8,128)S(1)} %get-tuple-element.15, f32[32,4,8]{0,2,1:T(8,128)S(1)} %get-tuple-element.14), channel_id=1, replica_groups=mesh['grp'=2,'tp'=16] {'tp'}, use_global_device_ids=true, to_apply=%region_4.5 | all-reduce | flops 2048 | bytes 16384 | tf_op jit(solution)/shard_map/psum | solution.py:109
  140.9 1.8 fusion.57
  142.8 0.9 constant_dynamic-slice_fusion
  143.6 58.3 %reduce-scatter.3.cloned.1.call-done = f32[32,4,256]{2,0,1:T(8,128)} async-done(((f32[32,4,4096]{2,0,1:T(8,128)}), f32[32,4,256]{2,0,1:T(8,128)}) %reduce-scatter.3.cloned.1.call-update) | async-done | bytes 131088 | tf_op jit(solution)/shard_map/reduce_scatter | solution.py:123
  201.9 1.5 add_convert_fusion.1
  203.8 36.5 %all-gather.2.cloned.1.call-done = bf16[32,4,4096]{2,0,1:T(8,128)(2,1)} async-done(((bf16[32,4,256]{2,0,1:T(8,128)(2,1)}), bf16[32,4,4096]{2,0,1:T(8,128)(2,1)}) %all-gather.2.cloned.1.call-update) | async-done | bytes 1048592 | tf_op jit(solution)/shard_map/all_gather | solution.py:127
  240.3 1.5 fusion.13
  241.8 1.5 fusion.15
  243.4 0.8 copy.78
  244.5 1.7 convolution_convert_fusion
  246.2 1.7 convolution_convert_fusion.1
  248.0 0.4 convolution_convert_fusion.2
  248.4 0.4 convolution_convert_fusion.3
  249.1 21.5 %all_gather.19 = bf16[32,4,2048]{2,1,0:T(4,128)(2,1)S(1)} all-gather(bf16[32,4,128]{2,1,0:T(4,128)(2,1)S(1)} %bitcast.113), channel_id=1, replica_groups=mesh['grp'=2,'tp'=16] {'tp'}, dimensions={2}, use_global_device_ids=true | all-gather | bytes 557056 | tf_op jit(solution)/shard_map/all_gather | solution.py:91
  270.6 18.9 %all_gather.18 = bf16[32,4,2048]{2,1,0:T(4,128)(2,1)S(1)} all-gather(bf16[32,4,128]{2,1,0:T(4,128)(2,1)S(1)} %bitcast.112), channel_id=1, replica_groups=mesh['grp'=2,'tp'=16] {'tp'}, dimensions={2}, use_global_device_ids=true | all-gather | bytes 557056 | tf_op jit(solution)/shard_map/all_gather | solution.py:90
  289.6 1.0 copy.80
  291.0 0.5 multiply_subtract_fusion
  291.4 0.8 copy-done.8
  292.2 6.6 %fusion = f32[32,8,4,16]{3,2,1,0:T(4,128)} fusion(f32[2,32,8,16,256]{4,3,2,1,0:T(8,128)} %param.10, f32[32,4,8,128]{3,1,2,0:T(4,128)S(1)} %get-tuple-element.44, f32[32,4,8,128]{3,1,2,0:T(4,128)S(1)} %get-tuple-element.45), kind=kOutput, calls=%fused_computation.2 | convolution fusion | flops 50593792 | bytes 5308416 | tf_op jit(solution)/shard_map/bthd,bhed->bthe/dot_general | solution.py:101
  298.8 1.3 copy.83
  300.1 3.4 convolution_multiply_fusion
  303.5 1.0 fusion.35
  305.0 59.2 %all-reduce = (f32[32,4,8]{0,2,1:T(8,128)S(1)}, f32[32,4,8]{0,2,1:T(8,128)S(1)}) all-reduce(f32[32,4,8]{0,2,1:T(8,128)S(1)} %get-tuple-element.13, f32[32,4,8]{0,2,1:T(8,128)S(1)} %get-tuple-element.12), channel_id=1, replica_groups=mesh['grp'=2,'tp'=16] {'tp'}, use_global_device_ids=true, to_apply=%region_10.11 | all-reduce | flops 2048 | bytes 16384 | tf_op jit(solution)/shard_map/psum | solution.py:109
  364.4 1.8 fusion.58
  366.3 4.5 %fusion.7 = f32[1,32,8,16,256]{4,3,2,1,0:T(8,128)S(1)} fusion(f32[2,32,8,16,256]{4,3,2,1,0:T(8,128)} %param.10, f32[8]{0:T(128)S(1)} %multiply_exponential_fusion.1, f32[32,4,8,128]{3,1,2,0:T(4,128)S(1)} %copy-done.5, f32[32,4,8,128]{3,1,2,0:T(4,128)S(1)} %copy-done.3, f32[4,8]{0,1:T(8,128)S(1)} %copy.85, bf16[32,4,8,16]{3,2,1,0:T(8,128)(2,1)S(1)} %reshape.319), kind=kOutput, calls=%fused_computation.10 | convolution fusion | flops 52953088 | bytes 9470112 | tf_op jit(solution)/shard_map/bthe,bthd->bhed/dot_general | solution.py:105
  370.8 4.5 %fusion.3 = f32[1,32,8,16,256]{4,3,2,1,0:T(8,128)S(1)} fusion(f32[2,32,8,16,256]{4,3,2,1,0:T(8,128)} %param.10, f32[8]{0:T(128)S(1)} %multiply_exponential_fusion.1, f32[32,4,8,128]{3,1,2,0:T(4,128)S(1)} %copy-done.7, f32[32,4,8,128]{3,1,2,0:T(4,128)S(1)} %get-tuple-element.28, f32[4,8]{0,1:T(8,128)S(1)} %copy.85, bf16[32,4,8,16]{3,2,1,0:T(8,128)(2,1)S(1)} %reshape.329), kind=kOutput, calls=%fused_computation.5 | convolution fusion | flops 52953088 | bytes 9470112 | tf_op jit(solution)/shard_map/bthe,bthd->bhed/dot_general | solution.py:105
  375.3 4.4 %pad_maximum_fusion = f32[2,32,8,16,256]{4,3,2,1,0:T(8,128)} fusion(f32[1,32,8,16,256]{4,3,2,1,0:T(8,128)S(1)} %fusion.3, f32[1,32,8,16,256]{4,3,2,1,0:T(8,128)S(1)} %fusion.7), kind=kLoop, calls=%fused_computation | loop fusion | flops 2097152 | bytes 16777216 | tf_op jit(solution)/shard_map/stack | solution.py:129
  379.8 45.6 %reduce-scatter.5.cloned.1.call-done = f32[32,4,256]{2,0,1:T(8,128)} async-done(((f32[32,4,4096]{2,0,1:T(8,128)}), f32[32,4,256]{2,0,1:T(8,128)}) %reduce-scatter.5.cloned.1.call-update) | async-done | bytes 131088 | tf_op jit(solution)/shard_map/reduce_scatter | solution.py:123
  425.4 0.9 add_convert_fusion
  426.3 0.7 copy.88
  (61 shorter events, 4.5 us)
Async XLA Ops:
  7.2 194.8 %reduce-scatter.3.cloned.1.call-start = ((), (), s32[]{:S(2)}) async-start(), calls=%async_computation.2 | async-start | bytes 2228224 | tf_op jit(solution)/shard_map/reduce_scatter | solution.py:123
  12.9 1.9 copy-start.11
  59.9 12.4 %copy-start.2 = (f32[32,4,8,128]{3,1,2,0:T(4,128)}, f32[32,4,8,128]{3,1,2,0:T(4,128)S(1)}, u32[]{:S(2)}) copy-start(f32[32,4,8,128]{3,1,2,0:T(4,128)S(1)} %get-tuple-element.32) | copy-start | bytes 1572868
  59.9 12.4 %copy-start.4 = (f32[32,4,8,128]{3,1,2,0:T(4,128)}, f32[32,4,8,128]{3,1,2,0:T(4,128)S(1)}, u32[]{:S(2)}) copy-start(f32[32,4,8,128]{3,1,2,0:T(4,128)S(1)} %get-tuple-element.33) | copy-start | bytes 1572868
  79.6 1.9 copy-start.9
  142.7 97.6 %all-gather.2.cloned.1.call-start = ((), (), s32[]{:S(2)}) async-start(), calls=%async_computation.3 | async-start | bytes 1114112 | tf_op jit(solution)/shard_map/all_gather | solution.py:127
  203.5 221.9 %reduce-scatter.5.cloned.1.call-start = ((), (), s32[]{:S(2)}) async-start(), calls=%async_computation.4 | async-start | bytes 2228224 | tf_op jit(solution)/shard_map/reduce_scatter | solution.py:123
  244.5 3.5 copy-start
  246.2 2.2 copy-start.1
  291.4 0.8 copy-start.8
  291.4 8.7 %copy-start.6 = (f32[32,4,8,128]{3,1,2,0:T(4,128)}, f32[32,4,8,128]{3,1,2,0:T(4,128)S(1)}, u32[]{:S(2)}) copy-start(f32[32,4,8,128]{3,1,2,0:T(4,128)S(1)} %get-tuple-element.29) | copy-start | bytes 1572868
  303.5 60.8 %copy-start.10 = (f32[32,4,8,16]{0,3,2,1:T(8,128)S(1)}, f32[32,4,8,16]{0,3,2,1:T(8,128)}, u32[]{:S(2)}) copy-start(f32[32,4,8,16]{0,3,2,1:T(8,128)} %copy.80) | copy-start | bytes 196612
  364.4 2.0 copy-start.3
  364.4 1.9 copy-start.5
  366.3 4.5 %copy-start.7 = (f32[32,4,8,128]{3,1,2,0:T(4,128)S(1)}, f32[32,4,8,128]{3,1,2,0:T(4,128)}, u32[]{:S(2)}) copy-start(f32[32,4,8,128]{3,1,2,0:T(4,128)} %copy-done.6) | copy-start | bytes 1572868
Sparse Core Ops, SparseCore 0:
  142.8 59.0 reduce-scatter.2
  204.7 35.5 all-gather.1
  366.3 58.9 reduce-scatter.4
where the time goes:
time: 434 us
  blocking collectives  202 us (47%)
  waiting for transfers between devices  140 us (32%)
  matrix products  41.1 us (9%)
  other arithmetic  17.9 us (4%)
  local copies, waits for them, and re-layouts  17.2 us (4%)
  between operations  14.2 us (3%)
    psum x2, blocking collectives, local(): lax.psum((jnp.sum(mixed, axis=-1), jnp.sum(mixed * mixed, axis=-1)), 'tp')  118 us
    reduce_scatter x2, waiting for transfers between devices, local(): lax.psum_scatter(partial_out, 'tp', scatter_dimension=2, tiled=True)  104 us
    all_gather x2, blocking collectives, local(): lax.all_gather(query_part, 'tp', axis=2, tiled=True)  43.5 us
    all_gather x2, blocking collectives, local(): lax.all_gather(key_part, 'tp', axis=2, tiled=True)  40.6 us
    all_gather x1, waiting for transfers between devices, local(): stream = lax.all_gather(stream_share, 'tp', axis=2, tiled=True)  36.5 us
    dot_general x2, matrix products, local(): jnp.einsum('bthd,bhed->bthe', rot_q, state, precision=highest)  13.5 us
    dot_general x2, matrix products, local(): jnp.einsum('bthe,bthd->bhed', values_f, rot_k * k_decay[None, :, :, None]...  8.98 us
  transfers between devices with their start and end apart: 3, of which 3 were waited for; matrix products, arithmetic and copies ran while one was open for 3% of the time, Pallas kernels for 0%

commit v1 on v0

--- a/solution.py
+++ b/solution.py
@@ -88,7 +88,7 @@
         gates_f = project_local(gate_weight[layer_no])
         queries, key_rows = (
             lax.all_gather(query_part, "tp", axis=2, tiled=True),
-            lax.all_gather(key_part, "tp", axis=2, tiled=True),
+            jnp.concatenate(lax.all_gather(key_part, "tp"), axis=2),
         )
         queries = queries.astype(jnp.float32).reshape(seqs, new_tok, heads, head_dim)
         key_rows = key_rows.astype(jnp.float32).reshape(seqs, new_tok, heads, head_dim)

time: 434 us -> 441 us (1.016)
  local copies, waits for them, and re-layouts: 17.2 us -> 22.3 us
where the time goes in v1:
time: 441 us; the launch traced here: 440 us
  blocking collectives  204 us (46%)
  waiting for transfers between devices  141 us (32%)
  matrix products  40.6 us (9%)
  local copies, waits for them, and re-layouts  22.3 us (5%)
  other arithmetic  18.6 us (4%)
  between operations  14.2 us (3%)
    psum x2, blocking collectives, local(): lax.psum((jnp.sum(mixed, axis=-1), jnp.sum(mixed * mixed, axis=-1)), 'tp')  118 us
    reduce_scatter x2, waiting for transfers between devices, local(): lax.psum_scatter(partial_out, 'tp', scatter_dimension=2, tiled=True)  104 us
    all_gather x2, blocking collectives, local(): lax.all_gather(query_part, 'tp', axis=2, tiled=True)  44.9 us
    all_gather x2, blocking collectives, local(): lax.all_gather(key_part, 'tp')  40.5 us
    all_gather x1, waiting for transfers between devices, local(): stream = lax.all_gather(stream_share, 'tp', axis=2, tiled=True)  36.7 us
    dot_general x2, matrix products, local(): jnp.einsum('bthd,bhed->bthe', rot_q, state, precision=highest)  12.8 us
    dot_general x2, matrix products, local(): jnp.einsum('bthe,bthd->bhed', values_f, rot_k * k_decay[None, :, :, None]...  8.98 us
  transfers between devices with their start and end apart: 3, of which 3 were waited for; matrix products, arithmetic and copies ran while one was open for 3% of the time, Pallas kernels for 0%

profile of v1, /device:TPU:0, one launch (start us, length us, event | category | flops | bytes accessed | tf_op | source)
XLA Modules:
  0.0 440.4 jit_solution(16511078269712216681)
XLA Ops:
  7.3 0.7 bitcast_convert_fusion
  8.0 1.8 fusion.10
  9.9 0.8 slice_convert_fusion
  10.7 1.9 fusion.12
  12.9 1.8 convolution_convert_fusion.4
  15.2 26.1 %all_gather.15 = bf16[32,4,2048]{2,1,0:T(4,128)(2,1)} all-gather(bf16[32,4,128]{2,1,0:T(4,128)(2,1)S(1)} %bitcast.115), channel_id=1, replica_groups=mesh['grp'=2,'tp'=16] {'tp'}, dimensions={2}, use_global_device_ids=true | all-gather | bytes 557056 | tf_op jit(solution)/shard_map/all_gather | solution.py:90
  41.3 19.0 %all_gather.16 = bf16[16,32,4,128]{3,1,2,0:T(8,128)(2,1)S(1)} all-gather(bf16[1,32,4,128]{3,1,2,0:T(8,128)(2,1)S(1)} %copy.96), channel_id=1, replica_groups=mesh['grp'=2,'tp'=16] {'tp'}, dimensions={0}, use_global_device_ids=true | all-gather | bytes 557056 | tf_op jit(solution)/shard_map/all_gather | solution.py:91
  60.4 0.6 copy.97
  61.5 0.9 copy-done.9
  62.7 0.6 multiply_subtract_fusion.2
  63.3 6.9 %fusion.4 = f32[32,8,4,16]{3,2,1,0:T(4,128)} fusion(f32[2,32,8,16,256]{4,3,2,1,0:T(8,128)} %param.10, f32[32,4,8,128]{3,1,2,0:T(4,128)S(1)} %get-tuple-element.50, f32[32,4,8,128]{3,1,2,0:T(4,128)S(1)} %get-tuple-element.51), kind=kOutput, calls=%fused_computation.7 | convolution fusion | flops 50593792 | bytes 5308416 | tf_op jit(solution)/shard_map/bthd,bhed->bthe/dot_general | solution.py:101
  70.3 2.0 copy.102
  72.3 2.7 fusion.56
  75.7 2.3 convolution_multiply_fusion.1
  78.0 1.0 fusion.38
  79.3 2.7 fusion.55
  82.0 0.4 convolution_convert_fusion.7
  83.0 1.8 fusion.54
  85.0 59.1 %all-reduce.1 = (f32[32,4,8]{0,2,1:T(8,128)S(1)}, f32[32,4,8]{0,2,1:T(8,128)S(1)}) all-reduce(f32[32,4,8]{0,2,1:T(8,128)S(1)} %get-tuple-element.15, f32[32,4,8]{0,2,1:T(8,128)S(1)} %get-tuple-element.14), channel_id=1, replica_groups=mesh['grp'=2,'tp'=16] {'tp'}, use_global_device_ids=true, to_apply=%region_4.5 | all-reduce | flops 2048 | bytes 16384 | tf_op jit(solution)/shard_map/psum | solution.py:109
  144.3 1.8 fusion.59
  146.4 0.9 constant_dynamic-slice_fusion
  147.3 58.1 %reduce-scatter.3.cloned.1.call-done = f32[32,4,256]{2,0,1:T(8,128)} async-done(((f32[32,4,4096]{2,0,1:T(8,128)}), f32[32,4,256]{2,0,1:T(8,128)}) %reduce-scatter.3.cloned.1.call-update) | async-done | bytes 131088 | tf_op jit(solution)/shard_map/reduce_scatter | solution.py:123
  205.3 1.5 add_convert_fusion.1
  207.0 36.7 %all-gather.2.cloned.1.call-done = bf16[32,4,4096]{2,0,1:T(8,128)(2,1)} async-done(((bf16[32,4,256]{2,0,1:T(8,128)(2,1)}), bf16[32,4,4096]{2,0,1:T(8,128)(2,1)}) %all-gather.2.cloned.1.call-update) | async-done | bytes 1048592 | tf_op jit(solution)/shard_map/all_gather | solution.py:127
  243.7 1.5 fusion.13
  245.2 1.5 fusion.15
  246.8 0.8 copy.104
  247.9 1.7 convolution_convert_fusion
  249.6 1.7 convolution_convert_fusion.1
  252.3 0.9 reshape.320
  253.2 21.5 %all_gather.19 = bf16[16,32,4,128]{3,1,2,0:T(8,128)(2,1)S(1)} all-gather(bf16[1,32,4,128]{3,1,2,0:T(8,128)(2,1)S(1)} %copy.107), channel_id=1, replica_groups=mesh['grp'=2,'tp'=16] {'tp'}, dimensions={0}, use_global_device_ids=true | all-gather | bytes 557056 | tf_op jit(solution)/shard_map/all_gather | solution.py:91
  274.7 18.9 %all_gather.18 = bf16[32,4,2048]{2,1,0:T(4,128)(2,1)S(1)} all-gather(bf16[32,4,128]{2,1,0:T(4,128)(2,1)S(1)} %bitcast.114), channel_id=1, replica_groups=mesh['grp'=2,'tp'=16] {'tp'}, dimensions={2}, use_global_device_ids=true | all-gather | bytes 557056 | tf_op jit(solution)/shard_map/all_gather | solution.py:90
  293.8 1.0 copy.106
  295.1 1.6 copy.108
  296.7 1.5 reshape.336
  298.3 1.3 multiply_subtract_fusion
  299.6 0.8 copy-done.10
  300.6 5.8 %fusion = f32[32,8,4,16]{3,2,1,0:T(4,128)S(1)} fusion(f32[2,32,8,16,256]{4,3,2,1,0:T(8,128)} %param.10, f32[32,4,8,128]{3,1,2,0:T(4,128)S(1)} %get-tuple-element.48, f32[32,4,8,128]{3,1,2,0:T(4,128)S(1)} %get-tuple-element.49), kind=kOutput, calls=%fused_computation.2 | convolution fusion | flops 50593792 | bytes 5308416 | tf_op jit(solution)/shard_map/bthd,bhed->bthe/dot_general | solution.py:101
  306.8 3.6 convolution_multiply_fusion
  310.3 1.0 fusion.35
  311.8 59.2 %all-reduce = (f32[32,4,8]{0,2,1:T(8,128)S(1)}, f32[32,4,8]{0,2,1:T(8,128)S(1)}) all-reduce(f32[32,4,8]{0,2,1:T(8,128)S(1)} %get-tuple-element.13, f32[32,4,8]{0,2,1:T(8,128)S(1)} %get-tuple-element.12), channel_id=1, replica_groups=mesh['grp'=2,'tp'=16] {'tp'}, use_global_device_ids=true, to_apply=%region_10.11 | all-reduce | flops 2048 | bytes 16384 | tf_op jit(solution)/shard_map/psum | solution.py:109
  371.2 1.8 fusion.60
  373.2 4.5 %fusion.7 = f32[1,32,8,16,256]{4,3,2,1,0:T(8,128)S(1)} fusion(f32[2,32,8,16,256]{4,3,2,1,0:T(8,128)} %param.10, f32[8]{0:T(128)S(1)} %multiply_exponential_fusion.1, f32[32,4,8,128]{3,1,2,0:T(4,128)S(1)} %copy-done.6, f32[32,4,8,128]{3,1,2,0:T(4,128)S(1)} %copy-done.4, f32[4,8]{0,1:T(8,128)S(1)} %copy.115, bf16[32,4,8,16]{3,2,1,0:T(8,128)(2,1)S(1)} %reshape.313), kind=kOutput, calls=%fused_computation.10 | convolution fusion | flops 52953088 | bytes 9470112 | tf_op jit(solution)/shard_map/bthe,bthd->bhed/dot_general | solution.py:105
  377.7 4.5 %fusion.3 = f32[1,32,8,16,256]{4,3,2,1,0:T(8,128)S(1)} fusion(f32[2,32,8,16,256]{4,3,2,1,0:T(8,128)} %param.10, f32[8]{0:T(128)S(1)} %multiply_exponential_fusion.1, f32[32,4,8,128]{3,1,2,0:T(4,128)S(1)} %copy-done.8, f32[32,4,8,128]{3,1,2,0:T(4,128)S(1)} %get-tuple-element.28, f32[4,8]{0,1:T(8,128)S(1)} %copy.115, bf16[32,4,8,16]{3,2,1,0:T(8,128)(2,1)S(1)} %copy-done.2), kind=kOutput, calls=%fused_computation.5 | convolution fusion | flops 52953088 | bytes 9470112 | tf_op jit(solution)/shard_map/bthe,bthd->bhed/dot_general | solution.py:105
  382.2 4.4 %pad_maximum_fusion = f32[2,32,8,16,256]{4,3,2,1,0:T(8,128)} fusion(f32[1,32,8,16,256]{4,3,2,1,0:T(8,128)S(1)} %fusion.3, f32[1,32,8,16,256]{4,3,2,1,0:T(8,128)S(1)} %fusion.7), kind=kLoop, calls=%fused_computation | loop fusion | flops 2097152 | bytes 16777216 | tf_op jit(solution)/shard_map/stack | solution.py:129
  386.6 45.6 %reduce-scatter.5.cloned.1.call-done = f32[32,4,256]{2,0,1:T(8,128)} async-done(((f32[32,4,4096]{2,0,1:T(8,128)}), f32[32,4,256]{2,0,1:T(8,128)}) %reduce-scatter.5.cloned.1.call-update) | async-done | bytes 131088 | tf_op jit(solution)/shard_map/reduce_scatter | solution.py:123
  432.2 0.9 add_convert_fusion
  433.2 0.7 copy.118
  (75 shorter events, 7.0 us)
Async XLA Ops:
  7.2 198.2 %reduce-scatter.3.cloned.1.call-start = ((), (), s32[]{:S(2)}) async-start(), calls=%async_computation.2 | async-start | bytes 2228224 | tf_op jit(solution)/shard_map/reduce_scatter | solution.py:123
  12.9 1.9 copy-start.14
  61.4 1.0 copy-start.9
  63.3 12.4 %copy-start.3 = (f32[32,4,8,128]{3,1,2,0:T(4,128)}, f32[32,4,8,128]{3,1,2,0:T(4,128)S(1)}, u32[]{:S(2)}) copy-start(f32[32,4,8,128]{3,1,2,0:T(4,128)S(1)} %get-tuple-element.32) | copy-start | bytes 1572868
  63.3 12.4 %copy-start.5 = (f32[32,4,8,128]{3,1,2,0:T(4,128)}, f32[32,4,8,128]{3,1,2,0:T(4,128)S(1)}, u32[]{:S(2)}) copy-start(f32[32,4,8,128]{3,1,2,0:T(4,128)S(1)} %get-tuple-element.33) | copy-start | bytes 1572868
  83.0 1.9 copy-start.12
  146.1 97.6 %all-gather.2.cloned.1.call-start = ((), (), s32[]{:S(2)}) async-start(), calls=%async_computation.3 | async-start | bytes 1114112 | tf_op jit(solution)/shard_map/all_gather | solution.py:127
  206.9 225.3 %reduce-scatter.5.cloned.1.call-start = ((), (), s32[]{:S(2)}) async-start(), calls=%async_computation.4 | async-start | bytes 2228224 | tf_op jit(solution)/shard_map/reduce_scatter | solution.py:123
  247.9 3.5 copy-start
  249.6 2.2 copy-start.1
  299.6 0.8 copy-start.10
  299.6 1.0 copy-start.11
  300.6 6.2 %copy-start.7 = (f32[32,4,8,128]{3,1,2,0:T(4,128)S(1)}, f32[32,4,8,128]{3,1,2,0:T(4,128)}, u32[]{:S(2)}) copy-start(f32[32,4,8,128]{3,1,2,0:T(4,128)} %get-tuple-element.29) | copy-start | bytes 1572868
  306.8 3.6 copy-start.2
  310.3 60.8 %copy-start.13 = (f32[32,4,8,16]{0,3,2,1:T(8,128)S(1)}, f32[32,4,8,16]{0,3,2,1:T(8,128)}, u32[]{:S(2)}) copy-start(f32[32,4,8,16]{0,3,2,1:T(8,128)} %copy.106) | copy-start | bytes 196612
  371.2 1.9 copy-start.4
  371.2 1.9 copy-start.6
  373.2 4.5 %copy-start.8 = (f32[32,4,8,128]{3,1,2,0:T(4,128)S(1)}, f32[32,4,8,128]{3,1,2,0:T(4,128)}, u32[]{:S(2)}) copy-start(f32[32,4,8,128]{3,1,2,0:T(4,128)} %get-tuple-element.29) | copy-start | bytes 1572868
Sparse Core Ops, SparseCore 0:
  146.2 59.0 reduce-scatter.2
  208.1 35.5 all-gather.1
  373.2 59.0 reduce-scatter.4
